TPU v7x, 256 devices: a 4x2x16 block of a 4x16x16 slice. The times are simulated.
256 devices in a mesh: grp: 2 (over y), sp: 32 (over z, core), tp: 4 (over x).
Axes of the slice: x: 4, y: 2, z: 16, core: 2. Of those that a mesh axis runs over, the one named last changes fastest.
The devices are a block of a 4x16x16 slice.
Arguments:
- residual: bfloat16 [16384, 2048], P(('grp', 'sp')), parts along dimension 0, may hold values from -6 to 6
- queries: bfloat16 [16384, 1024], P(('grp', 'sp'), 'tp'), parts along dimension 0, may hold values from -400 to 400
- keys: bfloat16 [16384, 1024], P(('grp', 'sp'), 'tp'), parts along dimension 0, may hold values from -8 to 8
- values: bfloat16 [16384, 1024], P(('grp', 'sp'), 'tp'), parts along dimension 0, may hold values from -6 to 6
- log_gates: float32 [16384, 16], P(('grp', 'sp'), 'tp'), parts along dimension 0, may hold values from -955 to 0, as said below
- w_out: bfloat16 [1024, 2048], P('tp'), may hold values from -0.75 to 0.75
- norm_gain: float32 [2048], replicated, may hold values from 0.1 to 1.9
- w_gate: bfloat16 [2048, 5632], P('sp', 'tp'), may hold values from -0.125 to 0.125
- w_up: bfloat16 [2048, 5632], P('sp', 'tp'), may hold values from -0.125 to 0.125
- w_down: bfloat16 [5632, 2048], P('tp', 'sp'), may hold values from -0.078125 to 0.078125
Outputs:
- output: bfloat16 [16384, 2048], P(('grp', 'sp', 'tp')), parts along dimension 0
There are 2 independent parts, one for each index of `grp`. A program takes and returns all parts, laid end to end along the dimension named above; an argument that names none is the same for every part. Nothing has to cross between parts.
Inputs may be any that keep to these rules, and one draw needn't show every extreme that they name: `log_gates`: never rises along positions.
All inputs are finite; a program needn't handle non-finite values.
Results may differ from a plain program's by a relative error of at most 0.014.
Values may be sent and summed in bfloat16 or wider, within the bound.
A program may use at most 128 MiB of HBM per device.

v0:
```python
import math
import jax
import jax.numpy as jnp
from jax import lax
from jax.sharding import PartitionSpec as P


def turned_gather(arrays, axis, dims):
    turned = [jnp.moveaxis(a, dim, 0) for a, dim in zip(arrays, dims)]
    widths = [t[0].size for t in turned]
    both = jnp.concatenate([t.reshape(-1, w) for t, w in zip(turned, widths)], axis=1)
    result = lax.all_gather(both, axis, axis=0, tiled=True)
    parts = jnp.split(result, [sum(widths[:k]) for k in range(1, len(widths))], axis=1)
    return tuple(
        (
            jnp.moveaxis(b.reshape(-1, *t.shape[1:]), 0, dim)
            for b, t, dim in zip(parts, turned, dims)
        )
    )


def cut_along(value, dim, peers):
    before, after = (value.shape[:dim], value.shape[dim + 1 :])
    return jnp.moveaxis(value.reshape(*before, peers, -1, *after), dim, 0)


def sent_and_summed(value, axis, dim):
    parts = cut_along(value, dim, lax.axis_size(axis))
    arrived = lax.all_to_all(parts, axis, split_axis=0, concat_axis=0, tiled=True)
    return arrived.astype(jnp.float32).sum(axis=0)


def sent_to_all(value, axis):
    copies = jnp.broadcast_to(value, (lax.axis_size(axis), *value.shape))
    return lax.all_to_all(copies, axis, split_axis=0, concat_axis=0, tiled=True)


def laid_out(parts, dim):
    parts = jnp.moveaxis(parts, 0, dim)
    dims = parts.shape
    return parts.reshape(*dims[:dim], dims[dim] * dims[dim + 1], *dims[dim + 2 :])


def gather_directly(value, axis, dim):
    parts = sent_to_all(value, axis)
    return laid_out(parts, dim)


def normalize(rows_in, gain):
    floats = rows_in.astype(jnp.float32)
    scaled = floats * lax.rsqrt(jnp.mean(floats * floats, axis=-1, keepdims=True) + 1e-06)
    return (scaled * gain).astype(jnp.bfloat16)


def attend(queries, keys, values, log_gates):
    row_count = queries.shape[0]
    head_count = log_gates.shape[1]
    head_width = queries.shape[1] // head_count
    score_scale = head_width ** (-0.5)
    first_row = lax.axis_index("sp") * row_count
    query_heads = queries.reshape(row_count, head_count, head_width)
    query_gates = log_gates.T
    query_positions = first_row + jnp.arange(row_count, dtype=jnp.int32)
    initial = (
        jnp.full((head_count, row_count), -1e30, jnp.float32),
        jnp.zeros((head_count, row_count), jnp.float32),
        jnp.zeros((head_count, row_count, head_width), jnp.float32),
    )
    carried = initial
    key_piece = lax.all_gather(keys.astype(jnp.float32), "sp", axis=0, tiled=True).astype(
        jnp.bfloat16
    )
    value_piece = lax.all_gather(values.astype(jnp.float32), "sp", axis=0, tiled=True).astype(
        jnp.bfloat16
    )
    gate_piece = lax.all_gather(log_gates, "sp", axis=0, tiled=True)
    length = key_piece.shape[0]
    block_rows = math.gcd(length, 2048)
    block_count = length // block_rows
    key_blocks = key_piece.reshape(block_count, block_rows, head_count, head_width)
    value_blocks = value_piece.reshape(block_count, block_rows, head_count, head_width)
    gate_blocks = gate_piece.reshape(block_count, block_rows, head_count)
    offsets = jnp.arange(block_count, dtype=jnp.int32) * block_rows

    def one_block(state, inputs):
        current_key_block, value_block, gate_block, offset = inputs

        def work(current):
            running_max, running_sum, accumulated = current
            scores = (
                jnp.einsum(
                    "qhd,khd->hqk",
                    query_heads,
                    current_key_block,
                    preferred_element_type=jnp.float32,
                )
                * score_scale
            )
            scores = scores + query_gates[:, :, None] - gate_block.T[:, None, :]
            key_positions = offset + jnp.arange(block_rows, dtype=jnp.int32)
            causal = (query_positions[:, None] >= key_positions[None, :])[None]
            scores = jnp.where(causal, scores, -1e30)
            new_max = jnp.maximum(running_max, jnp.max(scores, axis=-1))
            weights = jnp.where(causal, jnp.exp(scores - new_max[:, :, None]), 0.0)
            rescale = jnp.exp(running_max - new_max)
            running_sum = running_sum * rescale + jnp.sum(weights, axis=-1)
            product = jnp.einsum(
                "hqk,khd->hqd",
                weights.astype(jnp.bfloat16),
                value_block,
                preferred_element_type=jnp.float32,
            )
            accumulated = accumulated * rescale[:, :, None] + product
            return (new_max, running_sum, accumulated)

        state = lax.cond(offset <= first_row + row_count - 1, work, lambda current: current, state)
        return (state, None)

    carried, _ = lax.scan(one_block, carried, (key_blocks, value_blocks, gate_blocks, offsets))
    running_max, running_sum, accumulated = carried
    attended = accumulated / running_sum[:, :, None]
    return (
        attended.transpose(1, 0, 2).reshape(row_count, head_count * head_width).astype(jnp.bfloat16)
    )


def body(residual, queries, keys, values, log_gates, w_out, norm_gain, w_gate, w_up, w_down):
    gate_whole, up_whole, down_whole = turned_gather((w_gate, w_up, w_down), "sp", (0, 0, 1))
    attended = attend(queries, keys, values, log_gates)
    row_count = attended.shape[0]
    per_device = row_count // lax.axis_size("tp")
    my_first = lax.axis_index("tp") * per_device
    rows_part = attended
    projected = sent_and_summed(
        jnp.dot(rows_part, w_out, preferred_element_type=jnp.float32).astype(jnp.bfloat16), "tp", 0
    )
    own_rows = lax.dynamic_slice_in_dim(residual, my_first, per_device, 0)
    mixed = (own_rows.astype(jnp.float32) + projected).astype(jnp.bfloat16)
    normed_all = gather_directly(normalize(mixed, norm_gain), "tp", 0)
    gate_proj = jnp.dot(normed_all, gate_whole, preferred_element_type=jnp.float32)
    up_proj = jnp.dot(normed_all, up_whole, preferred_element_type=jnp.float32)
    hidden = (jax.nn.silu(gate_proj) * up_proj).astype(jnp.bfloat16)
    rows_part = hidden
    down_sum = sent_and_summed(
        jnp.dot(rows_part, down_whole, preferred_element_type=jnp.float32).astype(jnp.bfloat16),
        "tp",
        0,
    )
    summed = mixed.astype(jnp.float32) + 0.5 * down_sum
    scaled = summed * lax.rsqrt(jnp.mean(summed * summed, axis=-1, keepdims=True) + 1e-06)
    return scaled.astype(jnp.bfloat16)


def solution(mesh):
    in_specs = (
        P(("grp", "sp"), None),
        P(("grp", "sp"), "tp"),
        P(("grp", "sp"), "tp"),
        P(("grp", "sp"), "tp"),
        P(("grp", "sp"), "tp"),
        P("tp", None),
        P(),
        P("sp", "tp"),
        P("sp", "tp"),
        P("tp", "sp"),
    )
    out_specs = P(("grp", "sp", "tp"), None)
    return jax.shard_map(body, mesh=mesh, in_specs=in_specs, out_specs=out_specs, check_vma=False)
```

profile of v0, /device:TPU:33, one launch (start us, length us, event | category | flops | bytes accessed | tf_op | source)
XLA Modules:
  0.0 313.2 jit_solution(8759810375416187780)
XLA Ops:
  8.2 2.0 pad_maximum_fusion
  10.2 1.0 copy.15
  11.2 51.1 %all_gather.13 = f32[8192,4]{0,1:T(4,128)S(1)} all-gather(f32[256,4]{0,1:T(4,128)} %param.18), channel_id=1, replica_groups=mesh['grp'=2,'sp'=32,'tp'=4] {'sp'}, dimensions={0}, use_global_device_ids=true | all-gather | bytes 135168 | tf_op jit(solution)/shard_map/all_gather | solution.py:76
  62.3 33.5 %all-gather.4.cloned.1.call-done = bf16[8192,256]{1,0:T(8,128)(2,1)} async-done(((bf16[256,256]{1,0:T(8,128)(2,1)}), bf16[8192,256]{1,0:T(8,128)(2,1)}) %all-gather.4.cloned.1.call-update) | async-done | bytes 4194320 | tf_op jit(solution)/shard_map/all_gather | solution.py:70
  95.8 12.9 %reshape.83 = bf16[4,2048,4,64]{3,2,1,0:T(4,128)(2,1)} reshape(bf16[8192,256]{1,0:T(8,128)(2,1)} %all-gather.4.cloned.1.call-done) | data formatting | bytes 8388608 | tf_op jit(solution)/shard_map/reshape | solution.py:80
  108.7 12.9 %copy.17 = bf16[4,2048,4,64]{1,3,2,0:T(8,128)(2,1)} copy(bf16[4,2048,4,64]{3,2,1,0:T(4,128)(2,1)} %reshape.83) | data formatting | bytes 8388608
  121.6 45.0 %all-gather.6.cloned.1.call-done = bf16[8192,256]{1,0:T(8,128)(2,1)} async-done(((bf16[256,256]{1,0:T(8,128)(2,1)}), bf16[8192,256]{1,0:T(8,128)(2,1)}) %all-gather.6.cloned.1.call-update) | async-done | bytes 4194320 | tf_op jit(solution)/shard_map/all_gather | solution.py:73
  166.6 12.9 %reshape.84 = bf16[4,2048,4,64]{3,2,1,0:T(4,128)(2,1)} reshape(bf16[8192,256]{1,0:T(8,128)(2,1)} %all-gather.6.cloned.1.call-done) | data formatting | bytes 8388608 | tf_op jit(solution)/shard_map/reshape | solution.py:81
  179.5 13.0 %copy.18 = bf16[4,2048,4,64]{1,3,2,0:T(8,128)(2,1)} copy(bf16[4,2048,4,64]{3,2,1,0:T(4,128)(2,1)} %reshape.84) | data formatting | bytes 8388608
  192.5 18.0 %while.17 = (s32[]{:T(128)}, f32[4,256]{1,0:T(4,128)S(1)}, f32[4,256]{1,0:T(4,128)S(1)}, f32[4,256,64]{1,2,0:T(8,128)S(1)}, s32[4]{0:T(128)S(1)}, /*index=5*/s32...) while((s32[]{:T(128)}, f32[4,256]{1,0:T(4,128)S(1)}, ...), condition=%wide.region_5.6_spmd.clone, body=%wide.region_0.5_spmd.clone.sunk | while | flops 577376512 | bytes 30278972 | solution.py:119
  193.9 12.6 %conditional.3 = ((f32[4,256]{1,0:T(4,128)S(1)}, f32[4,256]{1,0:T(4,128)S(1)}, f32[4,256,64]{1,2,0:T(8,128)S(1)})) conditional(s32[]{:T(128)} %convert_element_type.112, (f32[4,256]{1,0:T(4,128)S(1)}, f32[4,256]{1,0:T(4,128)S(1)}, f32[4,256,64]{1,2,0:T(8,128)S(1)}) %tuple.48, (s32[]{:T(128)}, s32[]{:T(128)}, bf16[4,2048,4,64]{1,3,2,0:T(8,128)(2,1)}, ...), branch_computations={%region_1.1_spmd, %region_2.4_spmd} | conditional | flops 577376512 | bytes 30277676 | solution.py:116
  195.1 4.2 %fusion.4 = (f32[4,256]{1,0:T(4,128)S(1)}, f32[4,2048,256]{2,1,0:T(8,128)S(1)}) fusion(f32[4,2048]{1,0:T(4,128)S(1)} %dynamic-slice_bitcast_fusion, f32[4,256]{1,0:T(4,128)S(1)} %get-tuple-element.229, pred[256,2048]{0,1:T(8,128)(4,1)S(1)} %broadcast_compare_fusion, bf16[256,4,64]{0,2,1:T(8,128)(2,1)S(1)} %get-tuple-element.228, ...), kind=kOutput, calls=%fused_computation.5 | convolution fusion | flops 278920192 | bytes 10134016 | tf_op jit(solution)/shard_map/while/body/eval_jaxpr/cond/branch_1_fun/qhd,khd->hqk/dot_general | solution.py:91
  199.3 2.9 fusion.3
  202.3 4.2 %fusion.8 = f32[4,256,64]{1,2,0:T(8,128)S(1)} fusion(f32[4,2048,256]{2,1,0:T(8,128)S(1)} %get-tuple-element.328, f32[4,256]{1,0:T(4,128)S(1)} %max.4, f32[4,2048]{1,0:T(4,128)S(1)} %dynamic-slice_bitcast_fusion, f32[4,256]{1,0:T(4,128)S(1)} %get-tuple-element.229, pred[256,2048]{0,1:T(8,128)(4,1)S(1)} %broadcast_compare_fusion, ...), kind=kOutput, calls=%fused_computation.8 | convolution fusion | flops 283246592 | bytes 10531328 | tf_op jit(solution)/shard_map/while/body/eval_jaxpr/cond/branch_1_fun/hqk,khd->hqd/dot_general | solution.py:107
  210.6 1.4 convolution_convert_fusion
  212.1 3.7 %all-to-all-start = ((bf16[4,64,2048]{2,1,0:T(8,128)(2,1)}), bf16[4,64,2048]{2,1,0:T(8,128)(2,1)S(1)}, u32[]{:S(2)}, u32[]{:S(2)}) async-start(bf16[4,64,2048]{2,1,0:T(8,128)(2,1)} %bitcast.10), calls=%async_computation | async-start | bytes 2097152 | tf_op jit(solution)/shard_map/all_to_all | solution.py:29
  215.8 14.6 %all-to-all-done = bf16[4,64,2048]{2,1,0:T(8,128)(2,1)S(1)} async-done(((bf16[4,64,2048]{2,1,0:T(8,128)(2,1)}), bf16[4,64,2048]{2,1,0:T(8,128)(2,1)S(1)}, u32[]{:S(2)}, u32[]{:S(2)}) %all-to-all-start) | async-done | bytes 1048608 | tf_op jit(solution)/shard_map/all_to_all | solution.py:29
  230.5 1.1 fusion.44
  232.0 15.9 %all_to_all.15 = bf16[4,64,2048]{2,1,0:T(8,128)(2,1)S(1)} all-to-all(bf16[4,64,2048]{2,1,0:T(8,128)(2,1)S(1)} %broadcast_in_dim.51), channel_id=1, replica_groups=mesh['grp'=2,'sp'=32,'tp'=4] {'tp'}, dimensions={0} | all-to-all | bytes 2097152 | tf_op jit(solution)/shard_map/all_to_all | solution.py:35
  247.9 25.4 %all-gather.8.cloned.1.call-done = bf16[2048,4224]{1,0:T(8,128)(2,1)} async-done(((bf16[64,4224]{1,0:T(8,128)(2,1)}), bf16[2048,4224]{1,0:T(8,128)(2,1)}) %all-gather.8.cloned.1.call-update) | async-done | bytes 17301520 | tf_op jit(solution)/shard_map/all_gather | solution.py:12
  273.3 5.6 %fusion.25 = f32[256,1408]{1,0:T(8,128)} fusion(bf16[256,2048]{1,0:T(8,128)(2,1)S(1)} %bitcast.41, bf16[2048,4224]{1,0:T(8,128)(2,1)} %all-gather.8.cloned.1.call-done), kind=kOutput, calls=%fused_computation.29 | convolution fusion | flops 1476395008 | bytes 8257536 | tf_op jit(solution)/shard_map/dot_general | solution.py:140
  278.9 8.2 %fusion.33 = bf16[256,2048]{1,0:T(8,128)(2,1)S(1)} fusion(bf16[2048,4224]{1,0:T(8,128)(2,1)} %all-gather.8.cloned.1.call-done, bf16[256,2048]{1,0:T(8,128)(2,1)S(1)} %bitcast.42, f32[256,1408]{1,0:T(8,128)} %fusion.25), kind=kOutput, calls=%fused_computation.34 | convolution fusion | flops 2955476992 | bytes 15073280 | tf_op jit(solution)/shard_map/dot_general | solution.py:145
  287.0 18.4 %all_to_all.16 = bf16[4,64,2048]{2,1,0:T(8,128)(2,1)S(1)} all-to-all(bf16[4,64,2048]{2,1,0:T(8,128)(2,1)S(1)} %bitcast.43), channel_id=1, replica_groups=mesh['grp'=2,'sp'=32,'tp'=4] {'tp'}, dimensions={0} | all-to-all | bytes 2097152 | tf_op jit(solution)/shard_map/all_to_all | solution.py:29
  305.8 0.8 multiply_convert_fusion
  (42 shorter events, 6.3 us)
Async XLA Ops:
  6.5 204.1 %copy-start = (bf16[256,2048]{1,0:T(8,128)(2,1)S(1)}, bf16[256,2048]{1,0:T(8,128)(2,1)}, u32[]{:S(2)}) copy-start(bf16[256,2048]{1,0:T(8,128)(2,1)} %param.19) | copy-start | bytes 3145732
  6.6 89.2 %all-gather.4.cloned.1.call-start = ((), (), s32[]{:S(2)}) async-start(), calls=%async_computation.3 | async-start | bytes 4325376 | tf_op jit(solution)/shard_map/all_gather | solution.py:70
  7.3 159.3 %all-gather.6.cloned.1.call-start = ((), (), s32[]{:S(2)}) async-start(), calls=%async_computation.4 | async-start | bytes 4325376 | tf_op jit(solution)/shard_map/all_gather | solution.py:73
  8.1 265.2 %all-gather.8.cloned.1.call-start = ((), (), s32[]{:S(2)}) async-start(), calls=%async_computation.5 | async-start | bytes 17842176 | tf_op jit(solution)/shard_map/all_gather | solution.py:12
  179.5 13.0 %copy-start.1 = (f32[256,4]{0,1:T(4,128)S(1)}, f32[256,4]{0,1:T(4,128)}, u32[]{:S(2)}) copy-start(f32[256,4]{0,1:T(4,128)} %param.18) | copy-start | bytes 12292
  192.5 39.2 %copy-start.2 = (f32[2048]{0:T(1024)S(1)}, f32[2048]{0:T(1024)}, u32[]{:S(2)}) copy-start(f32[2048]{0:T(1024)} %param.20) | copy-start | bytes 24580
  212.1 18.3 %all-to-all-start = ((bf16[4,64,2048]{2,1,0:T(8,128)(2,1)}), bf16[4,64,2048]{2,1,0:T(8,128)(2,1)S(1)}, u32[]{:S(2)}, u32[]{:S(2)}) async-start(bf16[4,64,2048]{2,1,0:T(8,128)(2,1)} %bitcast.10), calls=%async_computation | async-start | bytes 2097152 | tf_op jit(solution)/shard_map/all_to_all | solution.py:29
Sparse Core Ops, SparseCore 0:
  9.2 86.5 all-gather.3
  97.6 68.9 all-gather.5
  168.4 104.8 all-gather.7
where the time goes:
time: 315 us; the launch traced here: 313 us
  waiting for transfers between devices  120 us (38%)
  blocking collectives  85.4 us (27%)
  local copies, waits for them, and re-layouts  55.5 us (18%)
  matrix products  23.6 us (7%)
  between operations  13.3 us (4%)
  other arithmetic  8.64 us (3%)
  starting transfers between devices  3.8 us (1%)
    all_gather x1, blocking collectives, attend(): gate_piece = lax.all_gather(log_gates, 'sp', axis=0, tiled=True)  51.1 us
    all_gather x1, waiting for transfers between devices, attend(): lax.all_gather(values.astype(jnp.float32), 'sp', axis=0, tiled=True)  45 us
    all_gather x1, waiting for transfers between devices, attend(): lax.all_gather(keys.astype(jnp.float32), 'sp', axis=0, tiled=True)  33.5 us
    unnamed x9, local copies, waits for them, and re-layouts  26.9 us
    all_gather x1, waiting for transfers between devices, turned_gather(): result = lax.all_gather(both, axis, axis=0, tiled=True)  25.4 us
    all_to_all x1, blocking collectives, sent_and_summed(): lax.all_to_all(parts, axis, split_axis=0, concat_axis=0, tiled=True)  18.4 us
    all_to_all x1, blocking collectives, sent_to_all(): return lax.all_to_all(copies, axis, split_axis=0, concat_axis=0, tiled=True)  15.9 us
    all_to_all x1, waiting for transfers between devices, sent_and_summed(): lax.all_to_all(parts, axis, split_axis=0, concat_axis=0, tiled=True)  14.6 us
  transfers between devices with their start and end apart: 4, of which 4 were waited for; matrix products, arithmetic and copies ran while one was open for 23% of the time, Pallas kernels for 0%

commit v1 on v0

--- a/solution.py
+++ b/solution.py
@@ -9,7 +9,9 @@
     turned = [jnp.moveaxis(a, dim, 0) for a, dim in zip(arrays, dims)]
     widths = [t[0].size for t in turned]
     both = jnp.concatenate([t.reshape(-1, w) for t, w in zip(turned, widths)], axis=1)
-    result = lax.all_gather(both, axis, axis=0, tiled=True)
+    result = jnp.concatenate(
+        lax.all_to_all(jnp.stack([both] * lax.axis_size(axis)), axis, 0, 0), axis=0
+    )
     parts = jnp.split(result, [sum(widths[:k]) for k in range(1, len(widths))], axis=1)
     return tuple(
         (

time: 315 us -> 1090 us (3.46)
  blocking collectives: 85.4 us -> 866 us
    all_to_all x1, blocking collectives: 15.9 us -> 797 us  [turned_gather(): lax.all_to_all(jnp.stack([both] * lax.axis_size(axis)), axis, 0, 0)]
    all_gather x1 -> x0, waiting for transfers between devices: 25.4 us -> none  [turned_gather(): result = lax.all_gather(both, axis, axis=0, tiled=True)]
    all_to_all x0 -> x1, waiting for transfers between devices: none -> 13.6 us  [sent_to_all(): return lax.all_to_all(copies, axis, split_axis=0, concat_axis=0, tiled=True)]
    unnamed x9 -> x17, local copies, waits for them, and re-layouts: 26.9 us -> 32.5 us
  transfers between devices with their start and end apart: 4 -> 4, of which waited for: 4 -> 4; matrix products, arithmetic and copies ran while one was open for 23% -> 2% of each run, Pallas kernels for 0% -> 0%
where the time goes in v1:
time: 1090 us
  blocking collectives  866 us (79%)
  waiting for transfers between devices  111 us (10%)
  local copies, waits for them, and re-layouts  63.8 us (6%)
  matrix products  21.9 us (2%)
  between operations  13.6 us (1%)
    all_to_all x1, blocking collectives, turned_gather(): lax.all_to_all(jnp.stack([both] * lax.axis_size(axis)), axis, 0, 0)  797 us
    all_gather x1, blocking collectives, attend(): gate_piece = lax.all_gather(log_gates, 'sp', axis=0, tiled=True)  51.1 us
    all_gather x1, waiting for transfers between devices, attend(): lax.all_gather(values.astype(jnp.float32), 'sp', axis=0, tiled=True)  45.4 us
    all_gather x1, waiting for transfers between devices, attend(): lax.all_gather(keys.astype(jnp.float32), 'sp', axis=0, tiled=True)  35.7 us
    unnamed x17, local copies, waits for them, and re-layouts  32.5 us
  transfers between devices with their start and end apart: 4, of which 4 were waited for; matrix products, arithmetic and copies ran while one was open for 2% of the time, Pallas kernels for 0%

profile of v1, /device:TPU:33, one launch (start us, length us, event | category | flops | bytes accessed | tf_op | source)
XLA Modules:
  0.0 1092.7 jit_solution(9073076486681802630)
XLA Ops:
  9.1 51.1 %all_gather.10 = f32[8192,4]{0,1:T(4,128)S(1)} all-gather(f32[256,4]{0,1:T(4,128)} %param.18), channel_id=1, replica_groups=mesh['grp'=2,'sp'=32,'tp'=4] {'sp'}, dimensions={0}, use_global_device_ids=true | all-gather | bytes 135168 | tf_op jit(solution)/shard_map/all_gather | solution.py:78
  60.3 35.7 %all-gather.3.cloned.1.call-done = bf16[8192,256]{1,0:T(8,128)(2,1)} async-done(((bf16[256,256]{1,0:T(8,128)(2,1)}), bf16[8192,256]{1,0:T(8,128)(2,1)}) %all-gather.3.cloned.1.call-update) | async-done | bytes 4194320 | tf_op jit(solution)/shard_map/all_gather | solution.py:72
  95.9 12.9 %reshape.89 = bf16[4,2048,4,64]{3,2,1,0:T(4,128)(2,1)} reshape(bf16[8192,256]{1,0:T(8,128)(2,1)} %all-gather.3.cloned.1.call-done) | data formatting | bytes 8388608 | tf_op jit(solution)/shard_map/reshape | solution.py:82
  108.9 12.8 %copy.17 = bf16[4,2048,4,64]{1,3,2,0:T(8,128)(2,1)} copy(bf16[4,2048,4,64]{3,2,1,0:T(4,128)(2,1)} %reshape.89) | data formatting | bytes 8388608
  121.6 45.4 %all-gather.5.cloned.1.call-done = bf16[8192,256]{1,0:T(8,128)(2,1)} async-done(((bf16[256,256]{1,0:T(8,128)(2,1)}), bf16[8192,256]{1,0:T(8,128)(2,1)}) %all-gather.5.cloned.1.call-update) | async-done | bytes 4194320 | tf_op jit(solution)/shard_map/all_gather | solution.py:75
  167.1 12.9 %reshape.90 = bf16[4,2048,4,64]{3,2,1,0:T(4,128)(2,1)} reshape(bf16[8192,256]{1,0:T(8,128)(2,1)} %all-gather.5.cloned.1.call-done) | data formatting | bytes 8388608 | tf_op jit(solution)/shard_map/reshape | solution.py:83
  180.0 12.7 %copy.18 = bf16[4,2048,4,64]{1,3,2,0:T(8,128)(2,1)} copy(bf16[4,2048,4,64]{3,2,1,0:T(4,128)(2,1)} %reshape.90) | data formatting | bytes 8388608
  192.8 17.2 %while.17 = (s32[]{:T(128)}, f32[4,256]{1,0:T(4,128)S(1)}, f32[4,256]{1,0:T(4,128)S(1)}, f32[4,256,64]{1,2,0:T(8,128)S(1)}, s32[4]{0:T(128)S(1)}, /*index=5*/s32...) while((s32[]{:T(128)}, f32[4,256]{1,0:T(4,128)S(1)}, ...), condition=%wide.region_5.6_spmd.clone, body=%wide.region_0.5_spmd.clone.sunk | while | flops 577376512 | bytes 30278980 | solution.py:121
  194.0 12.4 %conditional.3 = ((f32[4,256]{1,0:T(4,128)S(1)}, f32[4,256]{1,0:T(4,128)S(1)}, f32[4,256,64]{1,2,0:T(8,128)S(1)})) conditional(s32[]{:T(128)} %convert_element_type.112, (f32[4,256]{1,0:T(4,128)S(1)}, f32[4,256]{1,0:T(4,128)S(1)}, f32[4,256,64]{1,2,0:T(8,128)S(1)}) %tuple.48, (s32[]{:T(128)}, s32[]{:T(128)}, bf16[4,2048,4,64]{1,3,2,0:T(8,128)(2,1)}, ...), branch_computations={%region_1.1_spmd, %region_2.4_spmd} | conditional | flops 577376512 | bytes 30277676 | solution.py:118
  195.1 4.2 fusion.4
  199.2 2.9 fusion.3
  202.2 4.2 fusion.8
  210.0 1.4 convolution_convert_fusion
  211.5 3.9 all-to-all-start
  215.3 14.6 %all-to-all-done = bf16[4,64,2048]{2,1,0:T(8,128)(2,1)S(1)} async-done(((bf16[4,64,2048]{2,1,0:T(8,128)(2,1)}), bf16[4,64,2048]{2,1,0:T(8,128)(2,1)S(1)}, u32[]{:S(2)}, u32[]{:S(2)}) %all-to-all-start) | async-done | bytes 1048608 | tf_op jit(solution)/shard_map/all_to_all | solution.py:31
  230.1 1.1 fusion.44
  232.5 3.6 all-to-all-start.1
  236.2 13.6 %all-to-all-done.1 = bf16[4,64,2048]{2,1,0:T(8,128)(2,1)S(1)} async-done(((bf16[4,64,2048]{2,1,0:T(8,128)(2,1)}), bf16[4,64,2048]{2,1,0:T(8,128)(2,1)S(1)}, u32[]{:S(2)}, u32[]{:S(2)}) %all-to-all-start.1) | async-done | bytes 1048608 | tf_op jit(solution)/shard_map/all_to_all | solution.py:37
  249.8 2.1 stack.2
  251.9 796.6 %all_to_all.20 = bf16[32,64,4224]{2,1,0:T(8,128)(2,1)S(1)} all-to-all(bf16[32,64,4224]{2,1,0:T(8,128)(2,1)S(1)} %stack.2), channel_id=1, replica_groups=mesh['grp'=2,'sp'=32,'tp'=4] {'sp'}, dimensions={0} | all-to-all | bytes 34603008 | tf_op jit(solution)/shard_map/all_to_all | solution.py:13
  1048.4 5.9 copy-done.1
  1054.3 3.0 fusion.25
  1057.3 9.2 fusion.33
  1066.5 18.2 %all_to_all.21 = bf16[4,64,2048]{2,1,0:T(8,128)(2,1)S(1)} all-to-all(bf16[4,64,2048]{2,1,0:T(8,128)(2,1)} %bitcast.46), channel_id=1, replica_groups=mesh['grp'=2,'sp'=32,'tp'=4] {'tp'}, dimensions={0} | all-to-all | bytes 2097152 | tf_op jit(solution)/shard_map/all_to_all | solution.py:31
  (50 shorter events, 8.7 us)
Async XLA Ops:
  6.5 203.5 %copy-start = (bf16[256,2048]{1,0:T(8,128)(2,1)S(1)}, bf16[256,2048]{1,0:T(8,128)(2,1)}, u32[]{:S(2)}) copy-start(bf16[256,2048]{1,0:T(8,128)(2,1)} %param.19) | copy-start | bytes 3145732
  6.6 89.4 %all-gather.3.cloned.1.call-start = ((), (), s32[]{:S(2)}) async-start(), calls=%async_computation.4 | async-start | bytes 4325376 | tf_op jit(solution)/shard_map/all_gather | solution.py:72
  7.3 159.8 %all-gather.5.cloned.1.call-start = ((), (), s32[]{:S(2)}) async-start(), calls=%async_computation.5 | async-start | bytes 4325376 | tf_op jit(solution)/shard_map/all_gather | solution.py:75
  180.0 12.8 %copy-start.5 = (f32[256,4]{0,1:T(4,128)S(1)}, f32[256,4]{0,1:T(4,128)}, u32[]{:S(2)}) copy-start(f32[256,4]{0,1:T(4,128)} %param.18) | copy-start | bytes 12292
  192.8 38.5 %copy-start.6 = (f32[2048]{0:T(1024)S(1)}, f32[2048]{0:T(1024)}, u32[]{:S(2)}) copy-start(f32[2048]{0:T(1024)} %param.20) | copy-start | bytes 24580
  209.9 26.2 %copy-start.2 = (bf16[1408,64]{0,1:T(8,128)(2,1)S(1)}, bf16[1408,64]{0,1:T(8,128)(2,1)}, u32[]{:S(2)}) copy-start(bf16[1408,64]{0,1:T(8,128)(2,1)} %param.23) | copy-start | bytes 540676
  210.0 26.2 %copy-start.3 = (bf16[64,1408]{1,0:T(8,128)(2,1)S(1)}, bf16[64,1408]{1,0:T(8,128)(2,1)}, u32[]{:S(2)}) copy-start(bf16[64,1408]{1,0:T(8,128)(2,1)} %param.22) | copy-start | bytes 540676
  210.0 26.2 %copy-start.4 = (bf16[64,1408]{1,0:T(8,128)(2,1)S(1)}, bf16[64,1408]{1,0:T(8,128)(2,1)}, u32[]{:S(2)}) copy-start(bf16[64,1408]{1,0:T(8,128)(2,1)} %param.21) | copy-start | bytes 540676
  211.5 18.5 %all-to-all-start = ((bf16[4,64,2048]{2,1,0:T(8,128)(2,1)}), bf16[4,64,2048]{2,1,0:T(8,128)(2,1)S(1)}, u32[]{:S(2)}, u32[]{:S(2)}) async-start(bf16[4,64,2048]{2,1,0:T(8,128)(2,1)} %bitcast.10), calls=%async_computation | async-start | bytes 2097152 | tf_op jit(solution)/shard_map/all_to_all | solution.py:31
  232.5 17.3 %all-to-all-start.1 = ((bf16[4,64,2048]{2,1,0:T(8,128)(2,1)}), bf16[4,64,2048]{2,1,0:T(8,128)(2,1)S(1)}, u32[]{:S(2)}, u32[]{:S(2)}) async-start(bf16[4,64,2048]{2,1,0:T(8,128)(2,1)} %broadcast_in_dim.51), calls=%async_computation.1 | async-start | bytes 2097152 | tf_op jit(solution)/shard_map/all_to_all | solution.py:37
  1048.4 5.9 copy-start.1
Sparse Core Ops, SparseCore 0:
  9.2 86.6 all-gather.2
  97.8 69.2 all-gather.4
